TPU v7x, 32 devices: a whole 2x2x4 slice. The times are simulated.
32 devices in a mesh: grp: 2 (over y), sp: 4 (over z), tp: 4 (over x, core).
Axes of the slice: x: 2, y: 2, z: 4, core: 2. Of those that a mesh axis runs over, the one named last changes fastest.
Arguments:
- queries: bfloat16 [1024, 2048], P(('grp', 'sp'), 'tp'), parts along dimension 0, may hold values from -8 to 8
- keys: bfloat16 [1024, 1024], P(('grp', 'sp'), 'tp'), parts along dimension 0, may hold values from -6 to 6
- values: bfloat16 [1024, 1024], P(('grp', 'sp'), 'tp'), parts along dimension 0, may hold values from -6 to 6
- head_bias: float32 [16], P('tp'), may hold values from -15 to -5
- documents: int32 [1024], P(('grp', 'sp')), parts along dimension 0, may hold values from 0 to 2, never falling along the last dimension, each value on 1 to 384 neighbouring positions
- w_out: bfloat16 [2048, 2048], P('tp'), may hold values from -0.125 to 0.125
- resid: bfloat16 [1024, 2048], P(('grp', 'sp', 'tp')), parts along dimension 0, may hold values from -6 to 6
- norm_gain: float32 [2048], replicated, may hold values from 0.1 to 1.9
- expert_ids: int32 [1024, 2], P(('grp', 'sp', 'tp')), parts along dimension 0, may hold values from 0 to 3, all different within a row; in each aligned block of 32 rows (0 to 31, 32 to 63, ...) at most 32 rows name the same one
- expert_gates: float32 [1024, 2], P(('grp', 'sp', 'tp')), parts along dimension 0, may hold values from 0.1 to 0.9
- w_gate: bfloat16 [4, 2048, 3072], P('sp', None, 'tp'), may hold values from -0.125 to 0.125
- w_up: bfloat16 [4, 2048, 3072], P('sp', None, 'tp'), may hold values from -0.125 to 0.125
- w_down: bfloat16 [4, 3072, 2048], P('sp', 'tp'), may hold values from -0.109375 to 0.109375
Outputs:
- layer_out: bfloat16 [1024, 2048], P(('grp', 'sp', 'tp')), parts along dimension 0
There are 2 independent parts, one for each index of `grp`. A program takes and returns all parts, laid end to end along the dimension named above; an argument that names none is the same for every part. Nothing has to cross between parts.
Inputs may be any that keep to these rules, and one draw needn't show every extreme that they name: Document numbers never fall along the sequence; each of the 3 documents holds at least one position and the longest exactly 384 positions. `expert_ids`: each position names 2 different experts. Among the 32 positions of one device (aligned blocks of 32 rows) no expert is named more than 32 times, and in some block some expert exactly 32 times.
All inputs are finite; a program needn't handle non-finite values.
Results may differ from a plain program's by a relative error of at most 0.012.
Values may be sent and summed in bfloat16 or wider, within the bound.
A program may use at most 64 MiB of HBM per device.

v0:
```python
import functools

import jax
import jax.numpy as jnp
from jax import lax
from jax.experimental import pallas as pl
from jax.experimental.pallas import tpu as pltpu
from jax.sharding import PartitionSpec as P

D = 2048
HEADS = 16
KV_HEADS = 8
DH = 128
TOPK = 2


def passed_along(value, axis, steps):
    count = lax.axis_size(axis)
    initial, last = (max(0, -steps), min(count, count - steps))
    return lax.ppermute(value, axis, [(source, source + steps) for source in range(initial, last)])


def attend_terms(query_grid, bias_grid, key_block, value_block, live, carried):
    kv_local = bias_grid.shape[0]
    key_count = key_block.shape[0]
    logits = (
        jnp.einsum(
            "qgrd,sgd->grqs",
            query_grid,
            key_block.reshape(key_count, kv_local, DH),
            preferred_element_type=jnp.float32,
        )
        * DH ** (-0.5)
        + bias_grid[:, :, None, None]
    )
    keep = jnp.where(live, jax.nn.log_sigmoid(-logits), 0.0)
    after = lax.cumsum(keep, axis=3, reverse=True) - keep + carried[:, :, :, None]
    weight = jnp.where(live, jnp.exp(jax.nn.log_sigmoid(logits) + after), 0.0).astype(jnp.bfloat16)
    partial_mix = jnp.einsum(
        "grqs,sgd->qgrd",
        weight,
        value_block.reshape(key_count, kv_local, DH),
        preferred_element_type=jnp.float32,
    )
    return (partial_mix, jnp.sum(keep, axis=3))


def local(
    queries,
    keys,
    values,
    head_bias,
    documents,
    w_out,
    resid,
    norm_gain,
    expert_ids,
    expert_gates,
    w_gate,
    w_up,
    w_down,
):
    tok_count = queries.shape[0]
    kv_local = keys.shape[1] // DH
    group_size = HEADS // KV_HEADS
    sp_count = lax.axis_size("sp")
    tp_count = lax.axis_size("tp")
    sp_index = lax.axis_index("sp")
    query_grid = queries.reshape(tok_count, kv_local, group_size, DH)
    bias_grid = head_bias.reshape(kv_local, group_size)
    doc_here = documents.astype(jnp.bfloat16)
    doc_column = doc_here.reshape(tok_count, 1)
    local_pos = jnp.arange(tok_count, dtype=jnp.int32)
    live_local = (local_pos[None, :] < local_pos[:, None]) & (
        documents[None, :] == documents[:, None]
    )
    zero_carry = jnp.zeros((kv_local, group_size, tok_count), jnp.float32)
    mix_total, carried = attend_terms(query_grid, bias_grid, keys, values, live_local, zero_carry)

    def visit(turn_index, state):
        mix_sum, carry_sum, key_block, value_block, doc_block = state
        key_block, value_block, doc_block = passed_along(
            (key_block, value_block, doc_block), "sp", 1
        )
        live = (doc_block[:, 0][None, :] == doc_here[:, None]) & (sp_index - turn_index >= 0)
        partial_mix, block_keep = attend_terms(
            query_grid, bias_grid, key_block, value_block, live, carry_sum
        )
        return (mix_sum + partial_mix, carry_sum + block_keep, key_block, value_block, doc_block)

    mix_total, carried, key_last, value_last, doc_last = lax.fori_loop(
        1, sp_count, visit, (mix_total, carried, keys, values, doc_column)
    )
    mixed = mix_total.reshape(tok_count, kv_local * group_size * DH).astype(jnp.bfloat16)
    projected = lax.psum_scatter(
        jnp.dot(mixed, w_out, preferred_element_type=jnp.float32).astype(jnp.bfloat16),
        "tp",
        scatter_dimension=0,
        tiled=True,
    ).astype(jnp.float32)
    middle = (resid.astype(jnp.float32) + projected).astype(jnp.bfloat16)
    middle_value = middle.astype(jnp.float32)
    normed = (
        middle_value
        * lax.rsqrt(jnp.mean(middle_value * middle_value, axis=1, keepdims=True) + 1e-06)
        * norm_gain
    ).astype(jnp.bfloat16)
    row_count = normed.shape[0]
    expert_count = w_gate.shape[0] * sp_count
    slot_limit = min(row_count, max(2, 2 * TOPK * row_count // expert_count))
    flat_ids = expert_ids.reshape(-1)
    onehot_ids = (flat_ids[:, None] == jnp.arange(expert_count, dtype=jnp.int32)[None, :]).astype(
        jnp.int32
    )
    earlier = jnp.cumsum(onehot_ids, axis=0) - onehot_ids
    slot_ids = jnp.sum(earlier * onehot_ids, axis=1)
    target = flat_ids * slot_limit + slot_ids
    placing = (
        jnp.arange(expert_count * slot_limit, dtype=jnp.int32)[:, None] == target[None, :]
    ).astype(jnp.bfloat16)
    by_token = jnp.sum(placing.reshape(expert_count * slot_limit, row_count, TOPK), axis=2)
    outgoing = jnp.dot(by_token, normed, preferred_element_type=jnp.float32).astype(jnp.bfloat16)
    outgoing = outgoing.reshape(expert_count, slot_limit, D)
    arrived = lax.all_to_all(outgoing, "sp", split_axis=0, concat_axis=0, tiled=True)
    gathered = lax.all_gather(arrived, "tp", axis=0, tiled=True)
    expert_rows = gathered.reshape(-1, D)
    gate_value = jnp.dot(expert_rows, w_gate[0], preferred_element_type=jnp.float32)
    up_value = jnp.dot(expert_rows, w_up[0], preferred_element_type=jnp.float32)
    hidden = (jax.nn.silu(gate_value) * up_value).astype(jnp.bfloat16)
    partial_out = jnp.dot(hidden, w_down[0], preferred_element_type=jnp.float32)
    summed = lax.psum_scatter(
        partial_out.reshape(tp_count, sp_count * slot_limit, D).astype(jnp.bfloat16),
        "tp",
        scatter_dimension=0,
        tiled=True,
    ).astype(jnp.float32)
    expert_result = summed.reshape(sp_count, slot_limit, D).astype(jnp.bfloat16)
    returned = lax.all_to_all(expert_result, "sp", split_axis=0, concat_axis=0, tiled=True)
    routed = jnp.dot(placing.T, returned.reshape(-1, D), preferred_element_type=jnp.float32)
    combined = jnp.sum(expert_gates[:, :, None] * routed.reshape(row_count, TOPK, D), axis=1)
    return (middle_value + combined).astype(jnp.bfloat16)


MESH = pl.DeviceIdType.MESH


def paired(index, turn, count):
    result, bit = 0, 1
    while bit < count:
        a, b = lax.rem(index // bit, 2), lax.rem(turn // bit, 2)
        result = result + bit * (a + b - 2 * a * b)
        bit *= 2
    return result


def fused_kernel(
    sp_count,
    tp_count,
    q_ref,
    k_ref,
    v_ref,
    bias_ref,
    doc_ref,
    resid_ref,
    gain_ref,
    ids_ref,
    gates_ref,
    w_out_hbm,
    w_gate_hbm,
    w_up_hbm,
    w_down_hbm,
    out_ref,
    w_out,
    w_gate,
    w_up,
    w_down,
    k_all,
    v_all,
    doc_all,
    mix_acc,
    carry,
    mixed,
    middle,
    x_all,
    hidden,
    part,
    sib_in,
    x_out,
    x_in,
    z_out,
    returned,
    w_sem,
    kv_send,
    kv_recv,
    z_send,
    z_recv,
    gx_send,
    gx_recv,
    gs_send,
    gs_recv,
    ps_send,
    ps_recv,
    px_send,
    px_recv,
    rz_send,
    rz_recv,
):
    s = lax.axis_index("sp")
    t = lax.axis_index("tp")
    width = tp_count // 2
    x, c = t // 2, lax.rem(t, 2)
    sibling = 2 * x + 1 - c
    tok = q_ref.shape[0]
    kv_local = k_ref.shape[1] // DH
    rep = q_ref.shape[1] // k_ref.shape[1]
    rows, model = resid_ref.shape
    ff = w_up.shape[1]
    f32, bf16 = jnp.float32, jnp.bfloat16

    loads = [
        pltpu.make_async_copy(src, dst, w_sem.at[j])
        for j, (src, dst) in enumerate(
            (
                (w_out_hbm, w_out),
                (w_gate_hbm.at[0], w_gate),
                (w_up_hbm.at[0], w_up),
                (w_down_hbm.at[0], w_down),
            )
        )
    ]
    for load in loads:
        load.start()

    barrier = pltpu.get_barrier_semaphore()
    for j in range(1, sp_count):
        pl.semaphore_signal(
            barrier, inc=1, device_id={"sp": lax.rem(s + j, sp_count)}, device_id_type=MESH
        )
    for j in range(1, tp_count):
        pl.semaphore_signal(
            barrier, inc=1, device_id={"tp": lax.rem(t + j, tp_count)}, device_id_type=MESH
        )
    pl.semaphore_wait(barrier, sp_count + tp_count - 2)

    def remote(src, dst, send, recv, device):
        return pltpu.make_async_remote_copy(
            src_ref=src,
            dst_ref=dst,
            send_sem=send,
            recv_sem=recv,
            device_id=device,
            device_id_type=MESH,
        )

    lane_pieces = [slice(g * DH, (g + 1) * DH) for g in range(kv_local)]

    def passed(hop):
        right = {"sp": lax.rem(s + 1, sp_count)}
        pairs = [(doc_ref if hop == 0 else doc_all.at[hop - 1], doc_all.at[hop])]
        for own, slots in ((k_ref, k_all), (v_ref, v_all)):
            for lanes in lane_pieces:
                source = own.at[:, lanes] if hop == 0 else slots.at[hop - 1, :, lanes]
                pairs.append((source, slots.at[hop, :, lanes]))
        return [
            remote(src, dst, kv_send.at[hop, j], kv_recv.at[hop, j], right)
            for j, (src, dst) in enumerate(pairs)
        ]

    has_right = s < sp_count - 1

    @pl.when(has_right)
    def _():
        for copy in passed(0):
            copy.start()

    at_row = lax.broadcasted_iota(jnp.int32, (tok, tok), 0)
    at_col = lax.broadcasted_iota(jnp.int32, (tok, tok), 1)
    summing = jnp.concatenate(
        [(at_row > at_col).astype(f32), jnp.ones((tok, tok), f32)], axis=1
    ).astype(bf16)
    doc_query = jnp.broadcast_to(doc_ref[...].astype(f32), (tok, tok)).T

    def attend(hop):
        docs = doc_ref[...] if hop == 0 else doc_all[hop - 1]
        live = doc_query == jnp.broadcast_to(docs.astype(f32), (tok, tok))
        if hop == 0:
            live = live & (at_col < at_row)
        live_f = jnp.concatenate([live.astype(f32)] * rep, axis=0)
        live_all = live_f > 0.5
        for g in range(kv_local):
            heads = [g * rep + r for r in range(rep)]
            query = jnp.concatenate([q_ref[:, h * DH : (h + 1) * DH] for h in heads], axis=0)
            bias = jnp.concatenate([jnp.full((tok, tok), bias_ref[h], f32) for h in heads], axis=0)
            lanes = slice(g * DH, (g + 1) * DH)
            key = k_ref[:, lanes] if hop == 0 else k_all[hop - 1, :, lanes]
            value = v_ref[:, lanes] if hop == 0 else v_all[hop - 1, :, lanes]
            logits = (
                lax.dot_general(
                    query, key, (((1,), (1,)), ((), ())), preferred_element_type=f32
                )
                * DH ** (-0.5)
                + bias
            )
            keep_any = -(jnp.maximum(logits, 0.0) + jnp.log1p(jnp.exp(-jnp.abs(logits))))
            keep = jnp.where(live_all, keep_any, 0.0)
            high = keep.astype(bf16)
            rest = keep - high.astype(f32)
            mid = rest.astype(bf16)
            low = (rest - mid.astype(f32)).astype(bf16)
            sums = (
                jnp.dot(high, summing, preferred_element_type=f32)
                + jnp.dot(mid, summing, preferred_element_type=f32)
                + jnp.dot(low, summing, preferred_element_type=f32)
            )
            after, total = sums[:, :tok], sums[:, tok:]
            if hop > 0:
                after = after + carry[g]
                total = total + carry[g]
            carry[g] = total
            weight = jnp.where(live_all, jnp.exp(logits + keep_any + after), 0.0).astype(bf16)
            mix = jnp.dot(weight, value, preferred_element_type=f32)
            mix_acc[g] = mix if hop == 0 else mix_acc[g] + mix

    attend(0)
    for hop in range(1, sp_count):

        @pl.when(s >= hop)
        def _():
            onward = passed(hop) if hop < sp_count - 1 else None
            for j, copy in enumerate(passed(hop - 1)):
                copy.wait_recv()
                if onward is not None:
                    pl.when(has_right)(onward[j].start)

            attend(hop)

    for g in range(kv_local):
        for r in range(rep):
            h = g * rep + r
            mixed[:, h * DH : (h + 1) * DH] = mix_acc[g, r * tok : (r + 1) * tok, :].astype(bf16)

    cuts = 2
    span = model // cuts
    cols = [slice(h * span, (h + 1) * span) for h in range(cuts)]

    def pair_copies(i, h):
        return [
            remote(
                part.at[i, 2 * j + 1 - c, :, cols[h]],
                sib_in.at[i, j, :, cols[h]],
                ps_send.at[i, j, h],
                ps_recv.at[i, j, h],
                {"tp": sibling},
            )
            for j in range(width)
        ]

    def across_copies(i, h):
        return [
            remote(
                x_out.at[i, j - 1, :, cols[h]],
                x_in.at[i, j - 1, :, cols[h]],
                px_send.at[i, j - 1, h],
                px_recv.at[i, j - 1, h],
                {"tp": 2 * lax.rem(x + j, width) + c},
            )
            for j in range(1, width)
        ]

    def pair_sum(i, at, h):
        return part[i, 2 * at + c, :, cols[h]].astype(f32) + sib_in[i, at, :, cols[h]].astype(f32)

    def sum_pairs(i):
        for h in range(cuts):
            for copy in pair_copies(i, h):
                copy.wait_recv()
            for j, copy in enumerate(across_copies(i, h)):
                x_out[i, j, :, cols[h]] = pair_sum(i, lax.rem(x + j + 1, width), h).astype(bf16)
                copy.start()

    def sum_across(i, h):
        result = pair_sum(i, x, h)
        for j, copy in enumerate(across_copies(i, h)):
            copy.wait_recv()
            result = result + x_in[i, j, :, cols[h]].astype(f32)
        return result

    loads[0].wait()
    step = 512 if span % 512 == 0 else span
    steps = span // step

    def into_part(i, left, right):
        for h in range(cuts):

            def piece(n, _):
                columns = pl.ds(pl.multiple_of(n * step, step), step)
                value = jnp.dot(left[...], right[:, columns], preferred_element_type=f32)
                part[i, :, :, columns] = value.astype(bf16).reshape(tp_count, rows, step)
                return 0

            lax.fori_loop(h * steps, (h + 1) * steps, piece, 0)
            for copy in pair_copies(i, h):
                copy.start()

    into_part(sp_count, mixed, w_out)
    sum_pairs(sp_count)
    for h in range(cuts):
        middle[:, cols[h]] = (
            (resid_ref[:, cols[h]].astype(f32) + sum_across(sp_count, h)).astype(bf16).astype(f32)
        )
    mid_value = middle[...]
    x_all[s, t] = (
        mid_value
        * lax.rsqrt(jnp.mean(mid_value * mid_value, axis=1, keepdims=True) + 1e-06)
        * gain_ref[...]
    ).astype(bf16)

    def group(i):
        return paired(s, lax.rem(sp_count - i, sp_count), sp_count)

    def along_copy(i, h):
        block = x_all.at[s, t, :, cols[h]]
        return remote(block, block, z_send.at[i, h], z_recv.at[i, h], {"sp": group(i)})

    def spread_copies(i, h):
        block = x_all.at[group(i), t, :, cols[h]]
        return [
            remote(
                block,
                block,
                gx_send.at[i, j - 1, h],
                gx_recv.at[i, j - 1, h],
                {"tp": 2 * lax.rem(x + j, width) + c},
            )
            for j in range(1, width)
        ]

    def twin_copy(i, j, h):
        block = x_all.at[group(i), 2 * lax.rem(x - j + width, width) + c, :, cols[h]]
        return remote(block, block, gs_send.at[i, j, h], gs_recv.at[i, j, h], {"tp": sibling})

    def spread(i, h):
        for copy in spread_copies(i, h):
            copy.start()
        twin_copy(i, 0, h).start()

    def return_copy(i, h):
        return remote(
            z_out.at[i, :, cols[h]],
            returned.at[i, :, cols[h]],
            rz_send.at[i, h],
            rz_recv.at[i, h],
            {"sp": group(i)},
        )

    for h in range(cuts):
        for i in range(1, sp_count):
            along_copy(i, h).start()
        spread(0, h)
    for load in loads[1:]:
        load.wait()

    f_step = 256 if ff % 256 == 0 else ff

    def turn(i, _):
        @pl.when(i + 1 < sp_count)
        def _():
            for h in range(cuts):
                along_copy(i + 1, h).wait_recv()
                spread(i + 1, h)

        @pl.when(i < sp_count)
        def _():
            for h in range(cuts):
                for j, copy in enumerate(spread_copies(i, h)):
                    copy.wait_recv()
                    twin_copy(i, j + 1, h).start()
            for h in range(cuts):
                for j in range(width):
                    twin_copy(i, j, h).wait_recv()

        @pl.when(i < sp_count)
        def _():
            rows_in = x_all[group(i)].reshape(tp_count * rows, model)

            def widen(n, _):
                columns = pl.ds(pl.multiple_of(n * f_step, f_step), f_step)
                gate = jnp.dot(rows_in, w_gate[:, columns], preferred_element_type=f32)
                up = jnp.dot(rows_in, w_up[:, columns], preferred_element_type=f32)
                hidden[:, columns] = (gate / (1.0 + jnp.exp(-gate)) * up).astype(bf16)
                return 0

            lax.fori_loop(0, ff // f_step, widen, 0)
            into_part(i, hidden, w_down)

        @pl.when((i >= 1) & (i <= sp_count))
        def _():
            sum_pairs(i - 1)

        @pl.when(i >= 2)
        def _():
            for h in range(cuts):
                z_out[i - 2, :, cols[h]] = sum_across(i - 2, h).astype(bf16)
                pl.when(i > 2)(return_copy(i - 2, h).start)

        return 0

    lax.fori_loop(0, sp_count + 2, turn, 0)

    diagonal = lax.broadcasted_iota(jnp.int32, (rows, rows), 0) == lax.broadcasted_iota(
        jnp.int32, (rows, rows), 1
    )
    for i in range(sp_count):
        chosen = ids_ref[...] == group(i)
        gate_row = jnp.sum(jnp.where(chosen, gates_ref[...], 0.0), axis=0, keepdims=True)
        gate = jnp.sum(
            jnp.where(diagonal, jnp.broadcast_to(gate_row, (rows, rows)), 0.0), axis=1, keepdims=True
        )
        for h in range(cuts):
            if i > 0:
                return_copy(i, h).wait_recv()
            value = z_out[0, :, cols[h]] if i == 0 else returned[i, :, cols[h]]
            middle[:, cols[h]] = middle[:, cols[h]] + gate * value.astype(f32)
    out_ref[...] = middle[...].astype(bf16)

    for hop in range(sp_count - 1):

        @pl.when(has_right & (s >= hop))
        def _():
            for copy in passed(hop):
                copy.wait_send()

    def drain(i, _):
        for h in range(cuts):
            for copy in pair_copies(i, h) + across_copies(i, h):
                copy.wait_send()

            @pl.when(i < sp_count)
            def _():
                for copy in spread_copies(i, h):
                    copy.wait_send()
                for j in range(width):
                    twin_copy(i, j, h).wait_send()

            @pl.when((i >= 1) & (i < sp_count))
            def _():
                along_copy(i, h).wait_send()
                return_copy(i, h).wait_send()

        return 0

    lax.fori_loop(0, sp_count + 1, drain, 0)


def fused(
    queries,
    keys,
    values,
    head_bias,
    documents,
    w_out,
    resid,
    norm_gain,
    expert_ids,
    expert_gates,
    w_gate,
    w_up,
    w_down,
):
    sp_count, tp_count = lax.axis_size("sp"), lax.axis_size("tp")
    width = tp_count // 2
    tok = queries.shape[0]
    kv_local = keys.shape[1] // DH
    rep = queries.shape[1] // keys.shape[1]
    rows, model = resid.shape
    ff = w_up.shape[2]
    bf16, f32 = jnp.bfloat16, jnp.float32
    dma = pltpu.SemaphoreType.DMA
    vmem, hbm = pl.BlockSpec(memory_space=pltpu.VMEM), pl.BlockSpec(memory_space=pl.ANY)
    return pl.pallas_call(
        functools.partial(fused_kernel, sp_count, tp_count),
        out_shape=jax.ShapeDtypeStruct((rows, model), bf16),
        in_specs=[vmem] * 3
        + [pl.BlockSpec(memory_space=pltpu.SMEM)]
        + [vmem] * 5
        + [hbm] * 4,
        out_specs=vmem,
        scratch_shapes=[
            pltpu.VMEM(w_out.shape, bf16),
            pltpu.VMEM(w_gate.shape[1:], bf16),
            pltpu.VMEM(w_up.shape[1:], bf16),
            pltpu.VMEM(w_down.shape[1:], bf16),
            pltpu.VMEM((sp_count - 1,) + keys.shape, bf16),
            pltpu.VMEM((sp_count - 1,) + values.shape, bf16),
            pltpu.VMEM((sp_count - 1, 1, tok), jnp.int32),
            pltpu.VMEM((kv_local, rep * tok, DH), f32),
            pltpu.VMEM((kv_local, rep * tok, tok), f32),
            pltpu.VMEM(queries.shape, bf16),
            pltpu.VMEM((rows, model), f32),
            pltpu.VMEM((sp_count, tp_count, rows, model), bf16),
            pltpu.VMEM((tp_count * rows, ff), bf16),
            pltpu.VMEM((sp_count + 1, tp_count, rows, model), bf16),
            pltpu.VMEM((sp_count + 1, width, rows, model), bf16),
            pltpu.VMEM((sp_count + 1, width - 1, rows, model), bf16),
            pltpu.VMEM((sp_count + 1, width - 1, rows, model), bf16),
            pltpu.VMEM((sp_count, rows, model), bf16),
            pltpu.VMEM((sp_count, rows, model), bf16),
            dma((4,)),
            dma((sp_count - 1, 2 * kv_local + 1)),
            dma((sp_count - 1, 2 * kv_local + 1)),
            dma((sp_count, 2)),
            dma((sp_count, 2)),
            dma((sp_count, width - 1, 2)),
            dma((sp_count, width - 1, 2)),
            dma((sp_count, width, 2)),
            dma((sp_count, width, 2)),
            dma((sp_count + 1, width, 2)),
            dma((sp_count + 1, width, 2)),
            dma((sp_count + 1, width - 1, 2)),
            dma((sp_count + 1, width - 1, 2)),
            dma((sp_count, 2)),
            dma((sp_count, 2)),
        ],
        compiler_params=pltpu.CompilerParams(
            collective_id=0, has_side_effects=True, vmem_limit_bytes=60 * 2**20
        ),
    )(
        queries,
        keys,
        values,
        head_bias,
        documents.reshape(1, tok),
        resid,
        norm_gain.reshape(1, model),
        expert_ids.T,
        expert_gates.T,
        w_out,
        w_gate,
        w_up,
        w_down,
    )


def block(*arrays):
    queries, resid, w_gate = arrays[0], arrays[6], arrays[10]
    sp_count, tp_count = lax.axis_size("sp"), lax.axis_size("tp")
    rows = resid.shape[0]
    slots = min(rows, max(2, 2 * TOPK * rows // (w_gate.shape[0] * sp_count)))
    powers = sp_count & (sp_count - 1) == 0 and tp_count % 2 == 0 and min(sp_count, tp_count // 2) > 1
    if slots == rows and w_gate.shape[0] == 1 and powers and queries.shape[0] == DH:
        return fused(*arrays)
    return local(*arrays)


def solution(mesh):
    return jax.shard_map(
        block,
        mesh=mesh,
        in_specs=(
            P(("grp", "sp"), "tp"),
            P(("grp", "sp"), "tp"),
            P(("grp", "sp"), "tp"),
            P("tp"),
            P(("grp", "sp")),
            P("tp", None),
            P(("grp", "sp", "tp"), None),
            P(),
            P(("grp", "sp", "tp"), None),
            P(("grp", "sp", "tp"), None),
            P("sp", None, "tp"),
            P("sp", None, "tp"),
            P("sp", "tp", None),
        ),
        out_specs=P(("grp", "sp", "tp"), None),
        check_vma=False,
    )
```

profile of v0, /device:TPU:0, one launch (start us, length us, event | category | flops | bytes accessed | tf_op | source)
XLA Modules:
  0.0 66.9 jit_solution(6919049264007412089)
XLA Ops:
  0.0 65.3 %shard_map.127 = bf16[32,2048]{1,0:T(8,128)(2,1)} custom-call(bf16[128,512]{1,0:T(8,128)(2,1)} %q_ref.1, bf16[128,256]{1,0:T(8,128)(2,1)} %k_ref.1, bf16[128,256]{1,0:T(8,128)(2,1)} %v_ref.1, f32[4]{0:T(128)} %bias_ref.1, s32[1,128]{1,0:T(1,128)} %bitcast.7, bf16[32,2048]{1,0:T(8,128)(2,1)} %resid_ref.1, f32[1,2048]{1,0:T(1,128)} %bitcast.4, ...), custom_call_target="tpu_custom_call" | custom-call | tf_op jit(solution)/shard_map/pallas_call | solution.py:580
  65.3 1.6 %copy.15 = bf16[32,2048]{1,0:T(8,128)(2,1)} copy(bf16[32,2048]{1,0:T(8,128)(2,1)} %shard_map.127) | data formatting | bytes 262144
where the time goes:
time: 67 us; the launch traced here: 66.9 us
  Pallas kernels  65.3 us (97%)
  local copies, waits for them, and re-layouts  1.57 us (2%)
    pallas_call x1, Pallas kernels, fused(): pl.pallas_call(functools.partial(fused_kernel, sp_count, tp_count), out_s...  65.3 us
    unnamed x1, local copies, waits for them, and re-layouts  1.57 us

commit v1 on v0

--- a/solution.py
+++ b/solution.py
@@ -144,18 +144,35 @@
 MESH = pl.DeviceIdType.MESH
 
 
-def paired(index, turn, count):
-    result, bit = 0, 1
-    while bit < count:
-        a, b = lax.rem(index // bit, 2), lax.rem(turn // bit, 2)
-        result = result + bit * (a + b - 2 * a * b)
-        bit *= 2
-    return result
+def visiting_orders(count):
+    orders = []
+    for i in range(count):
+        order = [i] + [b for b in range(count) if b != i]
+        if i == count - 1:
+            order[:2] = order[1::-1]
+        if i == 0 and count > 3:
+            order[-2:] = order[:-3:-1]
+        orders.append(order)
+    return orders
 
 
 def fused_kernel(
     sp_count,
     tp_count,
+    q_hbm,
+    k_hbm,
+    v_hbm,
+    bias_hbm,
+    doc_hbm,
+    resid_hbm,
+    gain_hbm,
+    ids_hbm,
+    gates_hbm,
+    w_out_hbm,
+    w_gate_hbm,
+    w_up_hbm,
+    w_down_hbm,
+    out_ref,
     q_ref,
     k_ref,
     v_ref,
@@ -165,11 +182,6 @@
     gain_ref,
     ids_ref,
     gates_ref,
-    w_out_hbm,
-    w_gate_hbm,
-    w_up_hbm,
-    w_down_hbm,
-    out_ref,
     w_out,
     w_gate,
     w_up,
@@ -217,20 +229,6 @@
     ff = w_up.shape[1]
     f32, bf16 = jnp.float32, jnp.bfloat16
 
-    loads = [
-        pltpu.make_async_copy(src, dst, w_sem.at[j])
-        for j, (src, dst) in enumerate(
-            (
-                (w_out_hbm, w_out),
-                (w_gate_hbm.at[0], w_gate),
-                (w_up_hbm.at[0], w_up),
-                (w_down_hbm.at[0], w_down),
-            )
-        )
-    ]
-    for load in loads:
-        load.start()
-
     barrier = pltpu.get_barrier_semaphore()
     for j in range(1, sp_count):
         pl.semaphore_signal(
@@ -240,6 +238,29 @@
         pl.semaphore_signal(
             barrier, inc=1, device_id={"tp": lax.rem(t + j, tp_count)}, device_id_type=MESH
         )
+
+    moves = (
+        (doc_hbm, doc_ref),
+        (k_hbm, k_ref),
+        (v_hbm, v_ref),
+        (q_hbm, q_ref),
+        (bias_hbm, bias_ref),
+        (resid_hbm, resid_ref),
+        (gain_hbm, gain_ref),
+        (ids_hbm, ids_ref),
+        (gates_hbm, gates_ref),
+        (w_out_hbm, w_out),
+        (w_gate_hbm.at[0], w_gate),
+        (w_up_hbm.at[0], w_up),
+        (w_down_hbm.at[0], w_down),
+    )
+    loads = [
+        pltpu.make_async_copy(src, dst, w_sem.at[j]) for j, (src, dst) in enumerate(moves)
+    ]
+    for load in loads:
+        load.start()
+    for load in loads[:3]:
+        load.wait()
     pl.semaphore_wait(barrier, sp_count + tp_count - 2)
 
     def remote(src, dst, send, recv, device):
@@ -257,8 +278,8 @@
     def passed(hop):
         right = {"sp": lax.rem(s + 1, sp_count)}
         pairs = [(doc_ref if hop == 0 else doc_all.at[hop - 1], doc_all.at[hop])]
-        for own, slots in ((k_ref, k_all), (v_ref, v_all)):
-            for lanes in lane_pieces:
+        for lanes in lane_pieces:
+            for own, slots in ((k_ref, k_all), (v_ref, v_all)):
                 source = own.at[:, lanes] if hop == 0 else slots.at[hop - 1, :, lanes]
                 pairs.append((source, slots.at[hop, :, lanes]))
         return [
@@ -280,17 +301,19 @@
     ).astype(bf16)
     doc_query = jnp.broadcast_to(doc_ref[...].astype(f32), (tok, tok)).T
 
-    def attend(hop):
+    def live_keys(hop):
         docs = doc_ref[...] if hop == 0 else doc_all[hop - 1]
         live = doc_query == jnp.broadcast_to(docs.astype(f32), (tok, tok))
         if hop == 0:
             live = live & (at_col < at_row)
         live_f = jnp.concatenate([live.astype(f32)] * rep, axis=0)
-        live_all = live_f > 0.5
-        for g in range(kv_local):
+        return live_f > 0.5
+
+    def attend(hop, live_all, groups):
+        for g in groups:
             heads = [g * rep + r for r in range(rep)]
             query = jnp.concatenate([q_ref[:, h * DH : (h + 1) * DH] for h in heads], axis=0)
-            bias = jnp.concatenate([jnp.full((tok, tok), bias_ref[h], f32) for h in heads], axis=0)
+            bias = jnp.concatenate([jnp.broadcast_to(bias_ref[0:1, h : h + 1], (tok, tok)) for h in heads], axis=0)
             lanes = slice(g * DH, (g + 1) * DH)
             key = k_ref[:, lanes] if hop == 0 else k_all[hop - 1, :, lanes]
             value = v_ref[:, lanes] if hop == 0 else v_all[hop - 1, :, lanes]
@@ -321,19 +344,33 @@
             mix = jnp.dot(weight, value, preferred_element_type=f32)
             mix_acc[g] = mix if hop == 0 else mix_acc[g] + mix
 
-    attend(0)
+    for load in loads[3:5]:
+        load.wait()
+    groups = range(kv_local)
+    attend(0, live_keys(0), groups)
     for hop in range(1, sp_count):
 
-        @pl.when(s >= hop)
+        @pl.when(has_right & (s >= hop))
         def _():
             onward = passed(hop) if hop < sp_count - 1 else None
             for j, copy in enumerate(passed(hop - 1)):
                 copy.wait_recv()
                 if onward is not None:
-                    pl.when(has_right)(onward[j].start)
-
-            attend(hop)
-
+                    onward[j].start()
+            attend(hop, live_keys(hop), groups)
+
+        @pl.when(jnp.logical_not(has_right) & (s >= hop))
+        def _():
+            copies = passed(hop - 1)
+            copies[0].wait_recv()
+            live = live_keys(hop)
+            for g in groups:
+                copies[1 + 2 * g].wait_recv()
+                copies[2 + 2 * g].wait_recv()
+                attend(hop, live, [g])
+
+    for load in loads[5:10]:
+        load.wait()
     for g in range(kv_local):
         for r in range(rep):
             h = g * rep + r
@@ -385,7 +422,6 @@
             result = result + x_in[i, j, :, cols[h]].astype(f32)
         return result
 
-    loads[0].wait()
     step = 512 if span % 512 == 0 else span
     steps = span // step
 
@@ -402,8 +438,65 @@
             for copy in pair_copies(i, h):
                 copy.start()
 
+    def along_copy(b, h):
+        block = x_all.at[s, t, :, cols[h]]
+        return remote(block, block, z_send.at[b, h], z_recv.at[s, h], {"sp": b})
+
+    def along_arrival(b, h):
+        block = x_all.at[b, t, :, cols[h]]
+        return remote(block, block, z_send.at[b, h], z_recv.at[b, h], {"sp": b})
+
+    def spread_copies(b, h):
+        block = x_all.at[b, t, :, cols[h]]
+        return [
+            remote(
+                block,
+                block,
+                gx_send.at[b, j - 1, h],
+                gx_recv.at[b, j - 1, h],
+                {"tp": 2 * lax.rem(x + j, width) + c},
+            )
+            for j in range(1, width)
+        ]
+
+    def twin_copy(b, j, h):
+        block = x_all.at[b, 2 * lax.rem(x - j + width, width) + c, :, cols[h]]
+        return remote(block, block, gs_send.at[b, j, h], gs_recv.at[b, j, h], {"tp": sibling})
+
+    def spread(b, h):
+        for copy in spread_copies(b, h):
+            copy.start()
+        twin_copy(b, 0, h).start()
+
+    relayed = sp_count - 2 if sp_count > 3 else None
+
+    def relay_copy(b, h):
+        block = x_all.at[b, t, :, cols[h]]
+        return remote(block, block, z_send.at[s, h], z_recv.at[b, h], {"sp": 0})
+
+    def arrive(b):
+        for h in range(cuts):
+            along_arrival(b, h).wait_recv()
+            if b == relayed:
+                pl.when(s == 1)(relay_copy(b, h).start)
+            spread(b, h)
+
+    def return_copy(b, h):
+        return remote(
+            z_out.at[b, :, cols[h]],
+            returned.at[s, :, cols[h]],
+            rz_send.at[b, h],
+            rz_recv.at[s, h],
+            {"sp": b},
+        )
+
+    def return_arrival(e, h):
+        block = returned.at[e, :, cols[h]]
+        return remote(block, block, rz_send.at[e, h], rz_recv.at[e, h], {"sp": e})
+
     into_part(sp_count, mixed, w_out)
     sum_pairs(sp_count)
+    pl.when(s == sp_count - 1)(functools.partial(arrive, 0))
     for h in range(cuts):
         middle[:, cols[h]] = (
             (resid_ref[:, cols[h]].astype(f32) + sum_across(sp_count, h)).astype(bf16).astype(f32)
@@ -415,112 +508,97 @@
         * gain_ref[...]
     ).astype(bf16)
 
-    def group(i):
-        return paired(s, lax.rem(sp_count - i, sp_count), sp_count)
-
-    def along_copy(i, h):
-        block = x_all.at[s, t, :, cols[h]]
-        return remote(block, block, z_send.at[i, h], z_recv.at[i, h], {"sp": group(i)})
-
-    def spread_copies(i, h):
-        block = x_all.at[group(i), t, :, cols[h]]
-        return [
-            remote(
-                block,
-                block,
-                gx_send.at[i, j - 1, h],
-                gx_recv.at[i, j - 1, h],
-                {"tp": 2 * lax.rem(x + j, width) + c},
-            )
-            for j in range(1, width)
-        ]
-
-    def twin_copy(i, j, h):
-        block = x_all.at[group(i), 2 * lax.rem(x - j + width, width) + c, :, cols[h]]
-        return remote(block, block, gs_send.at[i, j, h], gs_recv.at[i, j, h], {"tp": sibling})
-
-    def spread(i, h):
-        for copy in spread_copies(i, h):
-            copy.start()
-        twin_copy(i, 0, h).start()
-
-    def return_copy(i, h):
-        return remote(
-            z_out.at[i, :, cols[h]],
-            returned.at[i, :, cols[h]],
-            rz_send.at[i, h],
-            rz_recv.at[i, h],
-            {"sp": group(i)},
-        )
-
+    def send_along(d):
+        for h in range(cuts):
+            along_copy(d, h).start()
+
+    for d in range(sp_count):
+        direct = (s != relayed) | (d > 0) if relayed else True
+        pl.when((d < s) & direct)(functools.partial(send_along, d))
+    for d in reversed(range(sp_count)):
+        pl.when(d > s)(functools.partial(send_along, d))
     for h in range(cuts):
-        for i in range(1, sp_count):
-            along_copy(i, h).start()
-        spread(0, h)
-    for load in loads[1:]:
+        spread(s, h)
+
+    for load in loads[10:]:
         load.wait()
 
     f_step = 256 if ff % 256 == 0 else ff
-
-    def turn(i, _):
-        @pl.when(i + 1 < sp_count)
-        def _():
-            for h in range(cuts):
-                along_copy(i + 1, h).wait_recv()
-                spread(i + 1, h)
-
-        @pl.when(i < sp_count)
-        def _():
-            for h in range(cuts):
-                for j, copy in enumerate(spread_copies(i, h)):
-                    copy.wait_recv()
-                    twin_copy(i, j + 1, h).start()
-            for h in range(cuts):
-                for j in range(width):
-                    twin_copy(i, j, h).wait_recv()
-
-        @pl.when(i < sp_count)
-        def _():
-            rows_in = x_all[group(i)].reshape(tp_count * rows, model)
-
-            def widen(n, _):
-                columns = pl.ds(pl.multiple_of(n * f_step, f_step), f_step)
-                gate = jnp.dot(rows_in, w_gate[:, columns], preferred_element_type=f32)
-                up = jnp.dot(rows_in, w_up[:, columns], preferred_element_type=f32)
-                hidden[:, columns] = (gate / (1.0 + jnp.exp(-gate)) * up).astype(bf16)
-                return 0
-
-            lax.fori_loop(0, ff // f_step, widen, 0)
-            into_part(i, hidden, w_down)
-
-        @pl.when((i >= 1) & (i <= sp_count))
-        def _():
-            sum_pairs(i - 1)
-
-        @pl.when(i >= 2)
-        def _():
-            for h in range(cuts):
-                z_out[i - 2, :, cols[h]] = sum_across(i - 2, h).astype(bf16)
-                pl.when(i > 2)(return_copy(i - 2, h).start)
-
+    orders = visiting_orders(sp_count)
+
+    def visited(u):
+        b = 0
+        for i in range(sp_count):
+            for j in range(sp_count):
+                b = jnp.where((s == i) & (u == j), orders[i][j], b)
+        return b
+
+    def finish(b):
+        for h in range(cuts):
+            z_out[b, :, cols[h]] = sum_across(b, h).astype(bf16)
+            pl.when(b != s)(return_copy(b, h).start)
+
+    def turn(u, _):
+        now, before = visited(u), visited(u - 1)
+        for i in range(sp_count):
+            ahead = 0 if i == 0 else 2 if i == sp_count - 1 else 1
+            for j, b in enumerate(orders[i]):
+                if b == i or (i == sp_count - 1 and b == 0):
+                    continue
+                at = max(0, min(j - ahead, sp_count - 2))
+                pl.when((s == i) & (u == at))(functools.partial(arrive, b))
+        pl.when((u > 0) & (u < sp_count - 1))(functools.partial(sum_pairs, before))
+        pl.when((u > 1) & (u < sp_count - 1))(functools.partial(finish, visited(u - 2)))
+        for h in range(cuts):
+            for j, copy in enumerate(spread_copies(now, h)):
+                copy.wait_recv()
+                twin_copy(now, j + 1, h).start()
+        pl.when(u == sp_count - 1)(functools.partial(sum_pairs, before))
+        for h in range(cuts):
+            for j in range(width):
+                twin_copy(now, j, h).wait_recv()
+
+        rows_in = x_all[now].reshape(tp_count * rows, model)
+
+        def widen(n, _):
+            columns = pl.ds(pl.multiple_of(n * f_step, f_step), f_step)
+            gate = jnp.dot(rows_in, w_gate[:, columns], preferred_element_type=f32)
+            up = jnp.dot(rows_in, w_up[:, columns], preferred_element_type=f32)
+            hidden[:, columns] = (gate / (1.0 + jnp.exp(-gate)) * up).astype(bf16)
+            return 0
+
+        lax.fori_loop(0, ff // f_step, widen, 0)
+        into_part(now, hidden, w_down)
         return 0
 
-    lax.fori_loop(0, sp_count + 2, turn, 0)
+    lax.fori_loop(0, sp_count, turn, 0)
+    finish(visited(sp_count - 3))
+    sum_pairs(visited(sp_count - 1))
+    finish(visited(sp_count - 2))
+    finish(visited(sp_count - 1))
 
     diagonal = lax.broadcasted_iota(jnp.int32, (rows, rows), 0) == lax.broadcasted_iota(
         jnp.int32, (rows, rows), 1
     )
-    for i in range(sp_count):
-        chosen = ids_ref[...] == group(i)
+    for e in range(sp_count):
+        chosen = ids_ref[...] == e
         gate_row = jnp.sum(jnp.where(chosen, gates_ref[...], 0.0), axis=0, keepdims=True)
         gate = jnp.sum(
             jnp.where(diagonal, jnp.broadcast_to(gate_row, (rows, rows)), 0.0), axis=1, keepdims=True
         )
-        for h in range(cuts):
-            if i > 0:
-                return_copy(i, h).wait_recv()
-            value = z_out[0, :, cols[h]] if i == 0 else returned[i, :, cols[h]]
-            middle[:, cols[h]] = middle[:, cols[h]] + gate * value.astype(f32)
+
+        @pl.when(e == s)
+        def _():
+            middle[...] = middle[...] + gate * z_out[s].astype(f32)
+
+        @pl.when(e != s)
+        def _():
+            for h in range(cuts):
+                return_arrival(e, h).wait_recv()
+                middle[:, cols[h]] = middle[:, cols[h]] + gate * returned[
+                    e, :, cols[h]
+                ].astype(f32)
+
     out_ref[...] = middle[...].astype(bf16)
 
     for hop in range(sp_count - 1):
@@ -542,10 +620,14 @@
                 for j in range(width):
                     twin_copy(i, j, h).wait_send()
 
-            @pl.when((i >= 1) & (i < sp_count))
+            @pl.when((i != s) & (i < sp_count))
             def _():
-                along_copy(i, h).wait_send()
                 return_copy(i, h).wait_send()
+
+            direct = (s != relayed) | (i > 0) if relayed else True
+            pl.when((i != s) & (i < sp_count) & direct)(along_copy(i, h).wait_send)
+            if relayed:
+                pl.when((i == s) & (s == 1))(relay_copy(relayed, h).wait_send)
 
         return 0
 
@@ -576,16 +658,28 @@
     ff = w_up.shape[2]
     bf16, f32 = jnp.bfloat16, jnp.float32
     dma = pltpu.SemaphoreType.DMA
-    vmem, hbm = pl.BlockSpec(memory_space=pltpu.VMEM), pl.BlockSpec(memory_space=pl.ANY)
+    operands = (
+        queries,
+        keys,
+        values,
+        head_bias.reshape(1, -1),
+        documents.reshape(1, tok),
+        resid,
+        norm_gain.reshape(1, model),
+        expert_ids.T,
+        expert_gates.T,
+        w_out,
+        w_gate,
+        w_up,
+        w_down,
+    )
     return pl.pallas_call(
         functools.partial(fused_kernel, sp_count, tp_count),
-        out_shape=jax.ShapeDtypeStruct((rows, model), bf16),
-        in_specs=[vmem] * 3
-        + [pl.BlockSpec(memory_space=pltpu.SMEM)]
-        + [vmem] * 5
-        + [hbm] * 4,
-        out_specs=vmem,
-        scratch_shapes=[
+        out_shape=pltpu.VMEM((rows, model), bf16),
+        in_specs=[pl.BlockSpec(memory_space=pl.ANY)] * len(operands),
+        out_specs=pl.BlockSpec(memory_space=pltpu.VMEM),
+        scratch_shapes=[pltpu.VMEM(one.shape, one.dtype) for one in operands[:9]]
+        + [
             pltpu.VMEM(w_out.shape, bf16),
             pltpu.VMEM(w_gate.shape[1:], bf16),
             pltpu.VMEM(w_up.shape[1:], bf16),
@@ -605,7 +699,7 @@
             pltpu.VMEM((sp_count + 1, width - 1, rows, model), bf16),
             pltpu.VMEM((sp_count, rows, model), bf16),
             pltpu.VMEM((sp_count, rows, model), bf16),
-            dma((4,)),
+            dma((13,)),
             dma((sp_count - 1, 2 * kv_local + 1)),
             dma((sp_count - 1, 2 * kv_local + 1)),
             dma((sp_count, 2)),
@@ -624,21 +718,7 @@
         compiler_params=pltpu.CompilerParams(
             collective_id=0, has_side_effects=True, vmem_limit_bytes=60 * 2**20
         ),
-    )(
-        queries,
-        keys,
-        values,
-        head_bias,
-        documents.reshape(1, tok),
-        resid,
-        norm_gain.reshape(1, model),
-        expert_ids.T,
-        expert_gates.T,
-        w_out,
-        w_gate,
-        w_up,
-        w_down,
-    )
+    )(*operands)
 
 
 def block(*arrays):
@@ -646,8 +726,8 @@
     sp_count, tp_count = lax.axis_size("sp"), lax.axis_size("tp")
     rows = resid.shape[0]
     slots = min(rows, max(2, 2 * TOPK * rows // (w_gate.shape[0] * sp_count)))
-    powers = sp_count & (sp_count - 1) == 0 and tp_count % 2 == 0 and min(sp_count, tp_count // 2) > 1
-    if slots == rows and w_gate.shape[0] == 1 and powers and queries.shape[0] == DH:
+    even = tp_count % 2 == 0 and sp_count > 2 and tp_count > 2
+    if slots == rows and w_gate.shape[0] == 1 and even and queries.shape[0] == DH:
         return fused(*arrays)
     return local(*arrays)
 

time: 67 us -> 56.7 us (0.85)
  the two profiles are of different devices: /device:TPU:0 before, /device:TPU:24 now
where the time goes in v1:
time: 56.7 us; the launch traced here: 56.6 us
  Pallas kernels  55.9 us (99%)
  local copies, waits for them, and re-layouts  0.66 us (1%)
    pallas_call x1, Pallas kernels, fused(): pl.pallas_call(functools.partial(fused_kernel, sp_count, tp_count), out_s...  55.9 us

profile of v1, /device:TPU:24, one launch (start us, length us, event | category | flops | bytes accessed | tf_op | source)
XLA Modules:
  0.0 56.6 jit_solution(11639640934988808340)
XLA Ops:
  0.0 55.9 %shard_map.127 = bf16[32,2048]{1,0:T(8,128)(2,1)S(1)} custom-call(bf16[128,512]{1,0:T(8,128)(2,1)} %q_hbm.1, bf16[128,256]{1,0:T(8,128)(2,1)} %k_hbm.1, bf16[128,256]{1,0:T(8,128)(2,1)} %v_hbm.1, f32[1,4]{1,0:T(1,128)} %bitcast.8, s32[1,128]{1,0:T(1,128)} %bitcast.9, bf16[32,2048]{1,0:T(8,128)(2,1)} %resid_hbm.1, f32[1,2048]{1,0:T(1,128)} %bitcast.5, ...), custom_call_target="tpu_custom_call" | custom-call | tf_op jit(solution)/shard_map/pallas_call | solution.py:676
  55.9 0.7 %copy.15 = bf16[32,2048]{1,0:T(8,128)(2,1)} copy(bf16[32,2048]{1,0:T(8,128)(2,1)S(1)} %shard_map.127) | data formatting | bytes 262144
